TPU v7x, 32 devices: a whole 2x2x4 slice. The times are simulated.
32 devices in a mesh: row: 4 (over y, x), col: 8 (over z, core).
Axes of the slice: x: 2, y: 2, z: 4, core: 2. Of those that a mesh axis runs over, the one named last changes fastest.
Arguments:
- mix_input: bfloat16 [4, 4096, 512], P(None, ('row', 'col')), may hold values from -6 to 6
- group_maps: bfloat16 [4, 128, 128], replicated, may hold values from -0.5 to 0.5
- out_map: bfloat16 [512, 2048], replicated, may hold values from -0.25 to 0.25
Outputs:
- mixed: bfloat16 [4, 4096, 2048], P(None, ('row', 'col'))
All inputs are finite; a program needn't handle non-finite values.
Results may differ from a plain program's by a relative error of at most 0.011.
Values may be sent and summed in bfloat16 or wider, within the bound.
A program may use at most 64 MiB of HBM per device.

v0:
```python
import math

import jax
import jax.numpy as jnp
from jax import lax
from jax.sharding import PartitionSpec as P

precise = lax.Precision.HIGHEST


def angle_pair(left_ids, right_ids, modulus):
    turn_count = left_ids[:, None] * right_ids[None, :] % modulus
    angles = turn_count.astype(jnp.float32) * (2.0 * math.pi / modulus)
    return (jnp.cos(angles), jnp.sin(angles))


def rotate(real_part, imag_part, cosine, sine_part):
    return (real_part * cosine + imag_part * sine_part, imag_part * cosine - real_part * sine_part)


def transform(real_in, imag_in, cosine, sine_part, einsum_form):
    real_out = jnp.einsum(einsum_form, real_in, cosine, precision=precise) + jnp.einsum(
        einsum_form, imag_in, sine_part, precision=precise
    )
    imag_out = jnp.einsum(einsum_form, imag_in, cosine, precision=precise) - jnp.einsum(
        einsum_form, real_in, sine_part, precision=precise
    )
    return (real_out, imag_out)


def per_device(mix_input, group_maps, out_map):
    sequences, positions, channels = mix_input.shape
    group_count, group_width, _ = group_maps.shape
    row_count = lax.axis_size("row")
    col_count = lax.axis_size("col")
    row_id = lax.axis_index("row")
    col_id = lax.axis_index("col")
    block_span = col_count * positions
    length = row_count * block_span
    norm_factor = 1.0 / math.sqrt(length * group_width)
    width_ids = jnp.arange(group_width, dtype=jnp.int32)
    real_tab, sine_tab = angle_pair(width_ids, width_ids, group_width)
    imag_tab = -sine_tab
    lane_count = real_tab.shape[1]
    signal = mix_input.astype(jnp.float32).reshape(sequences, positions, group_count, group_width)
    real_part = jnp.einsum("spgj,jl->sglp", signal, real_tab, precision=precise)
    imag_part = jnp.einsum("spgj,jl->sglp", signal, imag_tab, precision=precise)
    total_items = sequences * group_count * lane_count
    row_items = total_items // row_count
    dev_items = row_items // col_count
    send_shape = (row_count, row_items, 1, positions)
    col_shape = (col_count, dev_items, row_count, 1, positions)
    row_ids = jnp.arange(row_count, dtype=jnp.int32)
    pos_ids = jnp.arange(positions, dtype=jnp.int32)
    col_ids = jnp.arange(col_count, dtype=jnp.int32)
    row_cos, row_sin = angle_pair(row_ids, row_ids, row_count)
    turn_cos, turn_sin = angle_pair(row_ids, col_id * positions + pos_ids, length)
    col_cos, col_sin = angle_pair(col_ids, col_ids, col_count)
    step_cos, step_sin = angle_pair(col_ids, pos_ids, block_span)
    pos_cos, pos_sin = angle_pair(pos_ids, pos_ids, positions)
    row_send = (real_part.reshape(send_shape), imag_part.reshape(send_shape))
    pieces = (
        lax.all_to_all(row_send[0], "row", split_axis=0, concat_axis=2, tiled=True),
        lax.all_to_all(row_send[1], "row", split_axis=0, concat_axis=2, tiled=True),
    )
    spun_pair = transform(pieces[0][0], pieces[1][0], row_cos, row_sin, "nrp,rk->nkp")
    real_out, imag_out = rotate(spun_pair[0], spun_pair[1], turn_cos, turn_sin)
    real_rows = real_out[None]
    imag_rows = imag_out[None]
    pieces = (
        lax.all_to_all(
            real_rows.reshape(col_shape), "col", split_axis=0, concat_axis=3, tiled=True
        ),
        lax.all_to_all(
            imag_rows.reshape(col_shape), "col", split_axis=0, concat_axis=3, tiled=True
        ),
    )
    spun_pair = transform(pieces[0][0], pieces[1][0], col_cos, col_sin, "nacp,cb->nabp")
    turned = rotate(spun_pair[0], spun_pair[1], step_cos, step_sin)
    real_out = jnp.einsum("nabp,pq->nqba", turned[0], pos_cos, precision=precise) + jnp.einsum(
        "nabp,pq->nqba", turned[1], pos_sin, precision=precise
    )
    real_spec = real_out.reshape(1, real_out.shape[0], length)
    spectrum = real_spec[0][:, None]
    spectrum = (spectrum * norm_factor).astype(jnp.bfloat16)
    halves = spectrum.shape[1]
    spectrum = spectrum.reshape(1, dev_items, halves, row_count, col_count, positions)
    returned = lax.all_to_all(spectrum, "col", split_axis=4, concat_axis=0, tiled=True)
    held_groups = sequences * group_count // row_count
    returned = returned.reshape(held_groups, lane_count, halves, row_count, positions)
    full_width = returned[:, :, 0]
    group_ids = (row_id * held_groups + jnp.arange(held_groups, dtype=jnp.int32)) % group_count
    picker = (group_ids[:, None] == jnp.arange(group_count, dtype=jnp.int32)[None, :]).astype(
        jnp.bfloat16
    )
    chosen = jnp.einsum(
        "hg,glm->hlm", picker, group_maps, preferred_element_type=jnp.float32
    ).astype(jnp.bfloat16)
    grouped = jnp.einsum(
        "hlap,hlm->hapm", full_width, chosen, preferred_element_type=jnp.float32
    ).astype(jnp.bfloat16)
    grouped = grouped.reshape(1, held_groups, row_count, positions, group_width)
    arrived = lax.all_to_all(grouped, "row", split_axis=2, concat_axis=0, tiled=True)
    arrived = arrived.reshape(sequences, group_count, positions, group_width)
    mixed_out = jnp.einsum(
        "sgpm,gmn->spn",
        arrived,
        out_map.reshape(group_count, group_width, out_map.shape[1]),
        preferred_element_type=jnp.float32,
    )
    return mixed_out.astype(jnp.bfloat16)


def solution(mesh):
    return jax.shard_map(
        per_device,
        mesh=mesh,
        in_specs=(P(None, ("row", "col"), None), P(), P()),
        out_specs=P(None, ("row", "col"), None),
        check_vma=False,
    )
```

profile of v0, /device:TPU:0, one launch (start us, length us, event | category | flops | bytes accessed | tf_op | source)
XLA Modules:
  0.0 157.9 jit_solution(9652048484400523859)
XLA Ops:
  0.0 0.0 copy-start
  0.0 3.0 %fusion.30 = f32[128,4,128,4]{2,0,3,1:T(8,128)} fusion(bf16[4,128,512]{2,1,0:T(8,128)(2,1)} %param.3), kind=kOutput, calls=%fused_computation.42 | convolution fusion | flops 402882560 | bytes 1572864 | tf_op jit(solution)/shard_map/spgj,jl->sglp/dot_general | solution.py:46
  3.0 5.2 %all-to-all-start = ((f32[4,512,1,128]{3,1,2,0:T(8,128)}), f32[4,512,1,128]{3,1,2,0:T(8,128)S(1)}, u32[]{:S(2)}, u32[]{:S(2)}) async-start(f32[4,512,1,128]{3,1,2,0:T(8,128)} %bitcast.153), calls=%async_computation | async-start | bytes 2097152 | tf_op jit(solution)/shard_map/all_to_all | solution.py:63
  8.2 2.9 %fusion.28 = f32[128,4,128,4]{2,0,3,1:T(8,128)} fusion(bf16[4,128,512]{2,1,0:T(8,128)(2,1)} %param.3), kind=kOutput, calls=%fused_computation.40 | convolution fusion | flops 402898944 | bytes 1572864 | tf_op jit(solution)/shard_map/spgj,jl->sglp/dot_general | solution.py:47
  11.1 10.7 %all-to-all-done = f32[4,512,1,128]{3,1,2,0:T(8,128)S(1)} async-done(((f32[4,512,1,128]{3,1,2,0:T(8,128)}), f32[4,512,1,128]{3,1,2,0:T(8,128)S(1)}, u32[]{:S(2)}, u32[]{:S(2)}) %all-to-all-start) | async-done | bytes 1048608 | tf_op jit(solution)/shard_map/all_to_all | solution.py:63
  21.8 0.0 copy-start.1
  21.8 1.0 copy-done.1
  22.8 3.5 %all-to-all-start.1 = ((f32[4,512,1,128]{3,1,2,0:T(8,128)}), f32[4,512,1,128]{3,1,2,0:T(8,128)S(1)}, u32[]{:S(2)}, u32[]{:S(2)}) async-start(f32[4,512,1,128]{3,1,2,0:T(8,128)} %bitcast.152), calls=%async_computation.1 | async-start | bytes 2097152 | tf_op jit(solution)/shard_map/all_to_all | solution.py:64
  26.3 0.1 fusion.94
  26.4 4.6 %fusion.12 = f32[4,512,128]{2,0,1:T(4,128)} fusion(f32[4,512,1,128]{3,1,2,0:T(8,128)} %copy-done.1), kind=kOutput, calls=%fused_computation.20 | convolution fusion | flops 12583136 | bytes 2097152 | tf_op jit(solution)/shard_map/nrp,rk->nkp/dot_general | solution.py:22
  31.0 8.5 %all-to-all-done.1 = f32[4,512,1,128]{3,1,2,0:T(8,128)S(1)} async-done(((f32[4,512,1,128]{3,1,2,0:T(8,128)}), f32[4,512,1,128]{3,1,2,0:T(8,128)S(1)}, u32[]{:S(2)}, u32[]{:S(2)}) %all-to-all-start.1) | async-done | bytes 1048608 | tf_op jit(solution)/shard_map/all_to_all | solution.py:64
  39.5 0.0 copy-start.3
  39.5 2.4 %fusion.14 = f32[4,512,128]{2,0,1:T(4,128)S(1)} fusion(f32[4,512,1,128]{3,1,2,0:T(8,128)S(1)} %all-to-all-done.1), kind=kOutput, calls=%fused_computation.22 | convolution fusion | flops 12583136 | bytes 2097152 | tf_op jit(solution)/shard_map/nrp,rk->nkp/dot_general | solution.py:25
  41.8 0.0 copy-done.3
  41.8 0.0 copy-start.2
  41.8 2.5 %convolution_add_fusion.2 = f32[4,512,128]{2,0,1:T(4,128)S(1)} fusion(f32[4,512,128]{2,0,1:T(4,128)S(1)} %copy-done.3, f32[4,512,1,128]{3,1,2,0:T(8,128)S(1)} %all-to-all-done.1), kind=kOutput, calls=%fused_computation.6 | convolution fusion | flops 12845280 | bytes 3145728 | tf_op jit(solution)/shard_map/nrp,rk->nkp/dot_general | solution.py:22
  44.4 0.0 copy-done.2
  44.4 3.9 %multiply_add_fusion = (f32[4,512,128]{2,0,1:T(4,128)}, f32[4,512,128]{2,0,1:T(4,128)S(1)}) fusion(f32[4,512,128]{2,0,1:T(4,128)S(1)} %convolution_add_fusion.2, f32[4,128]{1,0:T(4,128)S(1)} %get-tuple-element.10, f32[4,128]{1,0:T(4,128)S(1)} %get-tuple-element.9, f32[4,512,128]{2,0,1:T(4,128)S(1)} %fusion.14, f32[4,512,1,128]{3,1,2,0:T(8,128)S(1)} %copy-done.2), kind=kOutput, calls=%fused_computation.31 | convolution fusion | flops 14418144 | bytes 5246976 | tf_op jit(solution)/shard_map/nrp,rk->nkp/dot_general | solution.py:25
  48.3 31.3 %all_to_all.90 = f32[8,64,4,1,128]{4,2,1,3,0:T(4,128)S(1)} all-to-all(f32[8,64,4,1,128]{4,2,1,3,0:T(4,128)S(1)} %bitcast.155), channel_id=1, replica_groups=mesh['row'=4,'col'=8] {'col'}, dimensions={0} | all-to-all | bytes 2097152 | tf_op jit(solution)/shard_map/all_to_all | solution.py:74
  79.5 4.4 %all-to-all-start.2 = ((f32[8,64,4,1,128]{4,2,1,3,0:T(4,128)}), f32[8,64,4,1,128]{4,2,1,3,0:T(4,128)}, u32[]{:S(2)}, u32[]{:S(2)}) async-start(f32[8,64,4,1,128]{4,2,1,3,0:T(4,128)} %bitcast.154), calls=%async_computation.2 | async-start | bytes 2097152 | tf_op jit(solution)/shard_map/all_to_all | solution.py:71
  84.0 0.1 fusion.82
  84.0 2.5 %fusion.8 = f32[8,64,4,128]{3,0,2,1:T(8,128)} fusion(f32[8,64,4,1,128]{4,2,1,3,0:T(4,128)S(1)} %all_to_all.90), kind=kOutput, calls=%fused_computation.16 | convolution fusion | flops 25166720 | bytes 2097152 | tf_op jit(solution)/shard_map/nacp,cb->nabp/dot_general | solution.py:25
  86.5 23.8 %all-to-all-done.2 = f32[8,64,4,1,128]{4,2,1,3,0:T(4,128)} async-done(((f32[8,64,4,1,128]{4,2,1,3,0:T(4,128)}), f32[8,64,4,1,128]{4,2,1,3,0:T(4,128)}, u32[]{:S(2)}, u32[]{:S(2)}) %all-to-all-start.2) | async-done | bytes 1048608 | tf_op jit(solution)/shard_map/all_to_all | solution.py:71
  110.4 0.0 copy-start.4
  110.4 2.8 %fusion.6 = f32[8,64,4,128]{3,0,2,1:T(8,128)S(1)} fusion(f32[8,64,4,1,128]{4,2,1,3,0:T(4,128)} %all-to-all-done.2), kind=kOutput, calls=%fused_computation.14 | convolution fusion | flops 25166720 | bytes 2097152 | tf_op jit(solution)/shard_map/nacp,cb->nabp/dot_general | solution.py:22
  113.2 0.0 copy-done.4
  113.2 2.7 %convolution_subtract_fusion = f32[8,64,4,128]{3,0,2,1:T(8,128)S(1)} fusion(f32[8,64,4,128]{3,0,2,1:T(8,128)S(1)} %copy-done.4, f32[8,64,4,1,128]{4,2,1,3,0:T(4,128)} %all-to-all-done.2), kind=kOutput, calls=%fused_computation.3 | convolution fusion | flops 25428864 | bytes 3145728 | tf_op jit(solution)/shard_map/nacp,cb->nabp/dot_general | solution.py:25
  115.9 1.7 %subtract_bitcast_fusion = (f32[64,4,8,128]{3,2,1,0:T(8,128)S(1)}, f32[64,4,8,128]{3,2,1,0:T(8,128)S(1)}) fusion(f32[8,64,4,128]{3,0,2,1:T(8,128)S(1)} %convolution_subtract_fusion, f32[8,128]{1,0:T(8,128)S(1)} %get-tuple-element.11, f32[8,128]{1,0:T(8,128)S(1)} %get-tuple-element.12, f32[8,64,4,128]{3,0,2,1:T(8,128)S(1)} %fusion.6, ...), kind=kOutput, calls=%fused_computation.28 | convolution fusion | flops 27001728 | bytes 5251072 | tf_op jit(solution)/shard_map/nacp,cb->nabp/dot_general | solution.py:22
  117.7 1.9 %fusion.18 = f32[128,64,4,8]{0,1,3,2:T(8,128)S(1)} fusion(f32[64,4,8,128]{3,2,1,0:T(8,128)S(1)} %get-tuple-element.6), kind=kOutput, calls=%fused_computation.26 | convolution fusion | flops 402882560 | bytes 2097152 | tf_op jit(solution)/shard_map/nabp,pq->nqba/dot_general | solution.py:80
  119.5 2.7 %fusion.3 = bf16[64,128,8,4]{1,0,2,3:T(8,128)(2,1)} fusion(f32[128,64,4,8]{0,1,3,2:T(8,128)S(1)} %fusion.18, f32[64,4,8,128]{3,2,1,0:T(8,128)S(1)} %get-tuple-element.5), kind=kOutput, calls=%fused_computation.10 | convolution fusion | flops 403668992 | bytes 2621440 | tf_op jit(solution)/shard_map/nabp,pq->nqba/dot_general | solution.py:80
  122.2 0.0 copy-start.5
  122.2 1.9 %copy.43 = bf16[64,128,8,4]{0,3,2,1:T(4,128)(2,1)S(1)} copy(bf16[64,128,8,4]{1,0,2,3:T(8,128)(2,1)} %fusion.3) | data formatting | bytes 1048576 | tf_op jit(solution)/shard_map/convert_element_type | solution.py:85
  124.1 1.1 copy.44
  125.2 3.5 %all-to-all-start.4 = ((bf16[1,64,1,4,8,128]{5,1,3,2,0,4:T(8,128)(2,1)}), bf16[1,64,1,4,8,128]{5,1,3,2,0,4:T(8,128)(2,1)S(1)}, u32[]{:S(2)}, u32[]{:S(2)}) async-start(bf16[1,64,1,4,8,128]{5,1,3,2,0,4:T(8,128)(2,1)} %copy.44), calls=%async_computation.4 | async-start | bytes 1048576 | tf_op jit(solution)/shard_map/all_to_all | solution.py:88
  128.7 0.0 copy-done.5
  128.7 0.3 fusion.4
  129.0 14.9 %all-to-all-done.4 = bf16[1,64,1,4,8,128]{5,1,3,2,0,4:T(8,128)(2,1)S(1)} async-done(((bf16[1,64,1,4,8,128]{5,1,3,2,0,4:T(8,128)(2,1)}), bf16[1,64,1,4,8,128]{5,1,3,2,0,4:T(8,128)(2,1)S(1)}, u32[]{:S(2)}, u32[]{:S(2)}) %all-to-all-start.4) | async-done | bytes 524320 | tf_op jit(solution)/shard_map/all_to_all | solution.py:88
  144.0 0.4 fusion.2
  144.4 10.9 %all_to_all.91 = bf16[1,4,4,128,128]{4,3,1,0,2:T(8,128)(2,1)S(1)} all-to-all(bf16[1,4,4,128,128]{4,3,1,0,2:T(8,128)(2,1)S(1)} %copy.49), channel_id=1, replica_groups=mesh['row'=4,'col'=8] {'row'}, dimensions={2} | all-to-all | bytes 1048576 | tf_op jit(solution)/shard_map/all_to_all | solution.py:103
  155.3 0.0 copy-done
  155.3 2.6 %bitcast_convert_fusion = bf16[4,128,2048]{2,1,0:T(8,128)(2,1)} fusion(bf16[4,128,2048,1]{2,1,3,0:T(8,128)(2,1)S(1)} %bitcast.150, bf16[1,4,4,128,128]{4,3,1,0,2:T(8,128)(2,1)S(1)} %all_to_all.91), kind=kOutput, calls=%fused_computation | convolution fusion | flops 1074790400 | bytes 4718592 | tf_op jit(solution)/shard_map/sgpm,gmn->spn/dot_general | solution.py:105
  (4 shorter events, 0.1 us)
Async XLA Ops:
  0.0 155.3 %copy-start = (bf16[512,2048]{1,0:T(8,128)(2,1)S(1)}, bf16[512,2048]{1,0:T(8,128)(2,1)}, u32[]{:S(2)}) copy-start(bf16[512,2048]{1,0:T(8,128)(2,1)} %param.5) | copy-start | bytes 6291460
  3.0 18.8 %all-to-all-start = ((f32[4,512,1,128]{3,1,2,0:T(8,128)}), f32[4,512,1,128]{3,1,2,0:T(8,128)S(1)}, u32[]{:S(2)}, u32[]{:S(2)}) async-start(f32[4,512,1,128]{3,1,2,0:T(8,128)} %bitcast.153), calls=%async_computation | async-start | bytes 2097152 | tf_op jit(solution)/shard_map/all_to_all | solution.py:63
  21.8 1.0 copy-start.1
  22.8 16.6 %all-to-all-start.1 = ((f32[4,512,1,128]{3,1,2,0:T(8,128)}), f32[4,512,1,128]{3,1,2,0:T(8,128)S(1)}, u32[]{:S(2)}, u32[]{:S(2)}) async-start(f32[4,512,1,128]{3,1,2,0:T(8,128)} %bitcast.152), calls=%async_computation.1 | async-start | bytes 2097152 | tf_op jit(solution)/shard_map/all_to_all | solution.py:64
  39.5 2.4 %copy-start.3 = (f32[4,512,128]{2,0,1:T(4,128)S(1)}, f32[4,512,128]{2,0,1:T(4,128)}, u32[]{:S(2)}) copy-start(f32[4,512,128]{2,0,1:T(4,128)} %fusion.12) | copy-start | bytes 3145732
  41.8 2.5 %copy-start.2 = (f32[4,512,1,128]{3,1,2,0:T(8,128)S(1)}, f32[4,512,1,128]{3,1,2,0:T(8,128)}, u32[]{:S(2)}) copy-start(f32[4,512,1,128]{3,1,2,0:T(8,128)} %copy-done.1) | copy-start | bytes 3145732
  79.5 30.8 %all-to-all-start.2 = ((f32[8,64,4,1,128]{4,2,1,3,0:T(4,128)}), f32[8,64,4,1,128]{4,2,1,3,0:T(4,128)}, u32[]{:S(2)}, u32[]{:S(2)}) async-start(f32[8,64,4,1,128]{4,2,1,3,0:T(4,128)} %bitcast.154), calls=%async_computation.2 | async-start | bytes 2097152 | tf_op jit(solution)/shard_map/all_to_all | solution.py:71
  110.4 2.8 %copy-start.4 = (f32[8,64,4,128]{3,0,2,1:T(8,128)S(1)}, f32[8,64,4,128]{3,0,2,1:T(8,128)}, u32[]{:S(2)}) copy-start(f32[8,64,4,128]{3,0,2,1:T(8,128)} %fusion.8) | copy-start | bytes 3145732
  122.2 6.5 %copy-start.5 = (bf16[4,128,128]{2,1,0:T(8,128)(2,1)S(1)}, bf16[4,128,128]{2,1,0:T(8,128)(2,1)}, u32[]{:S(2)}) copy-start(bf16[4,128,128]{2,1,0:T(8,128)(2,1)} %param.4) | copy-start | bytes 393220
  125.2 18.8 %all-to-all-start.4 = ((bf16[1,64,1,4,8,128]{5,1,3,2,0,4:T(8,128)(2,1)}), bf16[1,64,1,4,8,128]{5,1,3,2,0,4:T(8,128)(2,1)S(1)}, u32[]{:S(2)}, u32[]{:S(2)}) async-start(bf16[1,64,1,4,8,128]{5,1,3,2,0,4:T(8,128)(2,1)} %copy.44), calls=%async_computation.4 | async-start | bytes 1048576 | tf_op jit(solution)/shard_map/all_to_all | solution.py:88
where the time goes:
time: 159 us; the launch traced here: 158 us
  waiting for transfers between devices  58 us (36%)
  blocking collectives  42.2 us (27%)
  matrix products  36.8 us (23%)
  starting transfers between devices  16.6 us (10%)
  local copies, waits for them, and re-layouts  4.07 us (3%)
    all_to_all x1, blocking collectives, per_device(): lax.all_to_all(imag_rows.reshape(col_shape), 'col', split_axis=0, concat_...  31.3 us
    all_to_all x1, waiting for transfers between devices, per_device(): lax.all_to_all(real_rows.reshape(col_shape), 'col', split_axis=0, concat_...  23.8 us
    all_to_all x1, waiting for transfers between devices, per_device(): lax.all_to_all(spectrum, 'col', split_axis=4, concat_axis=0, tiled=True)  14.9 us
    all_to_all x1, blocking collectives, per_device(): lax.all_to_all(grouped, 'row', split_axis=2, concat_axis=0, tiled=True)  10.9 us
    all_to_all x1, waiting for transfers between devices, per_device(): lax.all_to_all(row_send[0], 'row', split_axis=0, concat_axis=2, tiled=True)  10.7 us
    all_to_all x1, waiting for transfers between devices, per_device(): lax.all_to_all(row_send[1], 'row', split_axis=0, concat_axis=2, tiled=True)  8.48 us
    dot_general x2, matrix products, transform(): jnp.einsum(einsum_form, real_in, cosine, precision=precise)  7.38 us
    dot_general x2, matrix products, transform(): jnp.einsum(einsum_form, real_in, sine_part, precision=precise)  6.61 us
  transfers between devices with their start and end apart: 4, of which 4 were waited for; matrix products, arithmetic and copies ran while one was open for 7% of the time, Pallas kernels for 0%

commit v1 on v0

v1 whole, which is shorter than its diff:
```python
import math

import jax
import jax.numpy as jnp
import numpy as np
from jax import lax
from jax.sharding import PartitionSpec as P

AXES = ("row", "col")


def turn_tables(left_count, right_count, modulus):
    turns = np.arange(left_count)[:, None] * np.arange(right_count)[None, :] % modulus
    angles = turns * (2.0 * math.pi / modulus)
    return np.cos(angles), np.sin(angles)


def lane_tables(width):
    cosine, sine = turn_tables(width, width, width)
    half = width // 2
    pack = np.zeros((width, width))
    unpack = np.zeros((width, width))
    pack[:, 0::2] = cosine[:, :half]
    pack[:, 1::2] = -sine[:, :half]
    pack[:, 1] = cosine[:, half]
    unpack[0, 0] = 1.0
    unpack[1, half] = 1.0
    for freq in range(1, half):
        unpack[2 * freq, freq] = unpack[2 * freq, width - freq] = 1.0
        unpack[2 * freq + 1, freq] = 1.0
        unpack[2 * freq + 1, width - freq] = -1.0
    return pack, unpack


def per_device(mix_input, group_maps, out_map):
    bf16, f32 = jnp.bfloat16, jnp.float32
    seqs, positions, channels = mix_input.shape
    groups, width, _ = group_maps.shape
    devices = lax.axis_size("row") * lax.axis_size("col")
    me = lax.axis_index("row") * lax.axis_size("col") + lax.axis_index("col")
    length = devices * positions
    items = seqs * channels // devices
    pack, unpack = lane_tables(width)

    lanes = jnp.einsum(
        "spgj,jc->sgcp",
        mix_input.reshape(seqs, positions, groups, width),
        jnp.asarray(pack, bf16),
        preferred_element_type=f32,
    ).astype(bf16)
    sent = lanes.reshape(devices, items, positions)
    held = lax.all_to_all(sent, AXES, split_axis=0, concat_axis=0, tiled=True)

    dev_cos, dev_sin = turn_tables(devices, devices, devices)
    both = jnp.asarray(np.concatenate([dev_cos, -dev_sin], axis=1), bf16)
    spun = jnp.einsum("df,dnp->fnp", both, held, preferred_element_type=f32)
    real_in, imag_in = spun[:devices], spun[devices:]
    twist_cos, twist_sin = turn_tables(devices, positions, length)
    twist_cos = jnp.asarray(twist_cos, f32)[:, None, :]
    twist_sin = jnp.asarray(twist_sin, f32)[:, None, :]
    real_part = real_in * twist_cos + imag_in * twist_sin
    imag_part = imag_in * twist_cos - real_in * twist_sin
    lane_ids = (me * items + jnp.arange(items, dtype=jnp.int32)) % width
    is_sine = ((lane_ids % 2 == 1) & (lane_ids != 1))[None, :, None]
    first = jnp.where(is_sine, -imag_part, real_part).astype(bf16)
    second = jnp.where(is_sine, real_part, imag_part).astype(bf16)
    stacked = jnp.concatenate([first, second], axis=2)
    pos_cos, pos_sin = turn_tables(positions, positions, positions)
    scale = 1.0 / math.sqrt(length * width)
    pos_table = jnp.asarray(np.concatenate([pos_cos, pos_sin], axis=0) * scale, bf16)
    freqs = jnp.einsum("pm,fnp->mfn", pos_table, stacked, preferred_element_type=f32).astype(bf16)

    freqs = freqs.reshape(devices, positions, items)
    back = lax.all_to_all(freqs, AXES, split_axis=0, concat_axis=0, tiled=True)
    parts = width // items
    back = back.reshape(seqs, groups, parts, positions, items)
    back = back.transpose(0, 3, 1, 2, 4).reshape(seqs * positions, groups, width)
    maps = jnp.einsum(
        "cl,glm->gcm", jnp.asarray(unpack, bf16), group_maps, preferred_element_type=f32
    ).astype(bf16)
    grouped = jnp.einsum("rgc,gcm->rgm", back, maps, preferred_element_type=f32).astype(bf16)
    mixed = jnp.dot(
        grouped.reshape(seqs * positions, channels), out_map, preferred_element_type=f32
    )
    return mixed.astype(bf16).reshape(seqs, positions, out_map.shape[1])


def solution(mesh):
    return jax.shard_map(
        per_device,
        mesh=mesh,
        in_specs=(P(None, AXES, None), P(), P()),
        out_specs=P(None, AXES, None),
        check_vma=False,
    )
```

time: 159 us -> 55.9 us (0.35)
  waiting for transfers between devices: 58 us -> 16.2 us
  matrix products: 36.8 us -> 7.93 us
  blocking collectives: 42.2 us -> 18.8 us
  starting transfers between devices: 16.6 us -> 7.32 us
    all_to_all x4 -> x1, waiting for transfers between devices: 58 us -> 16.2 us  [per_device(): held = lax.all_to_all(sent, AXES, split_axis=0, concat_axis=0, tiled=True)]
    dot_general x15 -> x5, matrix products: 36.8 us -> 7.93 us  [the longest x1 2.6 us: per_device(): jnp.dot(grouped.reshape(seqs * positions, channels), out_map, preferred_e...]
    all_to_all x2 -> x1, blocking collectives: 42.2 us -> 18.8 us  [per_device(): back = lax.all_to_all(freqs, AXES, split_axis=0, concat_axis=0, tiled=True)]
    all_to_all x4 -> x1, starting transfers between devices: 16.6 us -> 7.32 us  [per_device(): held = lax.all_to_all(sent, AXES, split_axis=0, concat_axis=0, tiled=True)]
  transfers between devices with their start and end apart: 4 -> 1, of which waited for: 4 -> 1; matrix products, arithmetic and copies ran while one was open for 7% -> 0% of each run, Pallas kernels for 0% -> 0%
where the time goes in v1:
time: 55.9 us; the launch traced here: 55.5 us
  blocking collectives  18.8 us (34%)
  waiting for transfers between devices  16.2 us (29%)
  matrix products  7.93 us (14%)
  starting transfers between devices  7.32 us (13%)
  local copies, waits for them, and re-layouts  4.48 us (8%)
  other arithmetic  0.59 us (1%)
    all_to_all x1, blocking collectives, per_device(): back = lax.all_to_all(freqs, AXES, split_axis=0, concat_axis=0, tiled=True)  18.8 us
    all_to_all x1, waiting for transfers between devices, per_device(): held = lax.all_to_all(sent, AXES, split_axis=0, concat_axis=0, tiled=True)  16.2 us
    all_to_all x1, starting transfers between devices, per_device(): held = lax.all_to_all(sent, AXES, split_axis=0, concat_axis=0, tiled=True)  7.32 us
    dot_general x1, matrix products, per_device(): jnp.dot(grouped.reshape(seqs * positions, channels), out_map, preferred_e...  2.6 us
    convert_element_type x1, local copies, waits for them, and re-layouts, per_device(): jnp.einsum('pm,fnp->mfn', pos_table, stacked, preferred_element_type=f32)  2.46 us
    dot_general x1, matrix products, per_device(): jnp.einsum('spgj,jc->sgcp', mix_input.reshape(seqs, positions, groups, wi...  2.31 us
    dot_general x1, matrix products, per_device(): jnp.einsum('pm,fnp->mfn', pos_table, stacked, preferred_element_type=f32)  2.05 us
    reshape x1, local copies, waits for them, and re-layouts, per_device(): freqs = freqs.reshape(devices, positions, items)  1.13 us
  transfers between devices with their start and end apart: 1, of which 1 were waited for; matrix products, arithmetic and copies ran while one was open for 0% of the time, Pallas kernels for 0%

profile of v1, /device:TPU:0, one launch (start us, length us, event | category | flops | bytes accessed | tf_op | source)
XLA Modules:
  0.0 55.5 jit_solution(3706394101566019626)
XLA Ops:
  0.0 0.0 copy-start
  0.0 0.0 copy-start.5
  0.0 2.3 %convolution_convert_fusion.3 = bf16[128,4,128,4]{2,0,3,1:T(8,128)(2,1)} fusion(bf16[128,128,1,1]{0,1,3,2:T(8,128)(2,1)} %constant.59, bf16[4,128,512]{2,1,0:T(8,128)(2,1)} %param.9), kind=kOutput, calls=%fused_computation.3 | convolution fusion | flops 67371008 | bytes 1081344 | tf_op jit(solution)/shard_map/spgj,jc->sgcp/dot_general | solution.py:45
  2.3 0.0 copy-start.3
  2.3 0.0 copy-start.4
  2.3 7.3 %all-to-all-start = ((bf16[32,64,128]{2,1,0:T(8,128)(2,1)}), bf16[32,64,128]{2,1,0:T(8,128)(2,1)S(1)}, u32[]{:S(2)}, u32[]{:S(2)}) async-start(bf16[32,64,128]{2,1,0:T(8,128)(2,1)} %bitcast.6), calls=%async_computation | async-start | bytes 1048576 | tf_op jit(solution)/shard_map/all_to_all | solution.py:52
  9.7 16.2 %all-to-all-done = bf16[32,64,128]{2,1,0:T(8,128)(2,1)S(1)} async-done(((bf16[32,64,128]{2,1,0:T(8,128)(2,1)}), bf16[32,64,128]{2,1,0:T(8,128)(2,1)S(1)}, u32[]{:S(2)}, u32[]{:S(2)}) %all-to-all-start) | async-done | bytes 524320 | tf_op jit(solution)/shard_map/all_to_all | solution.py:52
  25.9 0.0 copy-done.5
  25.9 0.5 fusion.5
  26.4 0.0 copy-done.3
  26.4 0.0 copy-done.4
  26.4 0.0 copy-start.6
  26.4 0.4 select_convert_fusion.1
  26.8 0.1 pad_maximum_fusion
  27.0 0.3 copy-done.6
  27.2 2.1 %fusion = bf16[128,32,64]{0,2,1:T(8,128)(2,1)} fusion(bf16[256,128,1]{1,0,2:T(8,128)(2,1)S(1)} %copy-done.6, bf16[32,64,256]{2,0,1:T(8,128)(2,1)S(1)} %pad_maximum_fusion), kind=kOutput, calls=%fused_computation.4 | convolution fusion | flops 134479872 | bytes 1638400 | tf_op jit(solution)/shard_map/pm,fnp->mfn/dot_general | solution.py:71
  29.3 2.5 %copy.23 = bf16[128,32,64]{2,1,0:T(8,128)(2,1)S(1)} copy(bf16[128,32,64]{0,2,1:T(8,128)(2,1)} %fusion) | data formatting | bytes 1048576 | tf_op jit(solution)/shard_map/convert_element_type | solution.py:71
  31.8 0.0 copy-start.1
  31.8 0.0 copy-start.2
  31.8 1.1 %copy.24 = bf16[32,128,64]{1,2,0:T(8,128)(2,1)} copy(bf16[32,128,64]{2,1,0:T(8,128)(2,1)S(1)} %bitcast.40) | data formatting | bytes 1048576 | tf_op jit(solution)/shard_map/reshape | solution.py:73
  32.9 18.8 %all_to_all.10 = bf16[32,128,64]{1,2,0:T(8,128)(2,1)S(1)} all-to-all(bf16[32,128,64]{1,2,0:T(8,128)(2,1)} %copy.24), channel_id=1, replica_groups=mesh['row'=4,'col'=8] {'row','col'}, dimensions={0} | all-to-all | bytes 1048576 | tf_op jit(solution)/shard_map/all_to_all | solution.py:74
  51.7 0.4 copy.25
  52.2 0.2 reshape.64
  52.4 0.0 copy-done.1
  52.4 0.0 copy-done.2
  52.4 0.5 convolution_convert_fusion.1
  52.9 0.0 copy-done
  52.9 2.6 %convolution_convert_fusion = bf16[512,2048]{1,0:T(8,128)(2,1)} fusion(bf16[512,512]{0,1:T(8,128)(2,1)S(1)} %bitcast.42, bf16[512,2048]{1,0:T(8,128)(2,1)S(1)} %copy-done), kind=kOutput, calls=%fused_computation | convolution fusion | flops 1074790400 | bytes 4718592 | tf_op jit(solution)/shard_map/dot_general | solution.py:82
  (1 shorter events, 0.0 us)
Async XLA Ops:
  0.0 52.9 %copy-start = (bf16[512,2048]{1,0:T(8,128)(2,1)S(1)}, bf16[512,2048]{1,0:T(8,128)(2,1)}, u32[]{:S(2)}) copy-start(bf16[512,2048]{1,0:T(8,128)(2,1)} %param.11) | copy-start | bytes 6291460
  0.0 25.9 %copy-start.5 = (bf16[32,64,1]{1,0,2:T(8,128)(2,1)S(1)}, bf16[32,64,1]{1,0,2:T(8,128)(2,1)}, u32[]{:S(2)}) copy-start(bf16[32,64,1]{1,0,2:T(8,128)(2,1)} %constant.58) | copy-start | bytes 12292
  2.3 24.1 %copy-start.3 = (f32[32,128]{1,0:T(8,128)S(1)}, f32[32,128]{1,0:T(8,128)}, u32[]{:S(2)}) copy-start(f32[32,128]{1,0:T(8,128)} %constant.54.clone) | copy-start | bytes 49156
  2.3 24.1 %copy-start.4 = (f32[32,128]{1,0:T(8,128)S(1)}, f32[32,128]{1,0:T(8,128)}, u32[]{:S(2)}) copy-start(f32[32,128]{1,0:T(8,128)} %constant.53.clone) | copy-start | bytes 49156
  2.3 23.6 %all-to-all-start = ((bf16[32,64,128]{2,1,0:T(8,128)(2,1)}), bf16[32,64,128]{2,1,0:T(8,128)(2,1)S(1)}, u32[]{:S(2)}, u32[]{:S(2)}) async-start(bf16[32,64,128]{2,1,0:T(8,128)(2,1)} %bitcast.6), calls=%async_computation | async-start | bytes 1048576 | tf_op jit(solution)/shard_map/all_to_all | solution.py:52
  26.4 0.8 %copy-start.6 = (bf16[256,128,1]{1,0,2:T(8,128)(2,1)S(1)}, bf16[256,128,1]{1,0,2:T(8,128)(2,1)}, u32[]{:S(2)}) copy-start(bf16[256,128,1]{1,0,2:T(8,128)(2,1)} %constant.60) | copy-start | bytes 196612
  31.8 20.6 %copy-start.1 = (bf16[4,128,128]{2,1,0:T(8,128)(2,1)S(1)}, bf16[4,128,128]{2,1,0:T(8,128)(2,1)}, u32[]{:S(2)}) copy-start(bf16[4,128,128]{2,1,0:T(8,128)(2,1)} %param.10) | copy-start | bytes 393220
  31.8 20.6 %copy-start.2 = (bf16[128,128,1]{1,0,2:T(8,128)(2,1)S(1)}, bf16[128,128,1]{1,0,2:T(8,128)(2,1)}, u32[]{:S(2)}) copy-start(bf16[128,128,1]{1,0,2:T(8,128)(2,1)} %constant.57) | copy-start | bytes 98308

commit v2 on v1

--- a/solution.py
+++ b/solution.py
@@ -4,6 +4,8 @@
 import jax.numpy as jnp
 import numpy as np
 from jax import lax
+from jax.experimental import pallas as pl
+from jax.experimental.pallas import tpu as pltpu
 from jax.sharding import PartitionSpec as P
 
 AXES = ("row", "col")
@@ -32,16 +34,193 @@
     return pack, unpack
 
 
-def per_device(mix_input, group_maps, out_map):
+def fourier(values):
+    count = len(values)
+    if count == 1:
+        return values
+    even, odd = fourier(values[0::2]), fourier(values[1::2])
+    low, high = [], []
+    for at in range(count // 2):
+        cosine = math.cos(2.0 * math.pi * at / count)
+        sine = math.sin(2.0 * math.pi * at / count)
+        (even_re, even_im), (odd_re, odd_im) = even[at], odd[at]
+        if at == 0:
+            turn_re, turn_im = odd_re, odd_im
+        elif 4 * at == count:
+            turn_re, turn_im = odd_im, -odd_re
+        elif odd_im is None:
+            turn_re, turn_im = odd_re * cosine, odd_re * -sine
+        else:
+            turn_re = odd_re * cosine + odd_im * sine
+            turn_im = odd_im * cosine - odd_re * sine
+        if turn_re is None:
+            low_re = high_re = even_re
+        else:
+            low_re, high_re = even_re + turn_re, even_re - turn_re
+        if turn_im is None:
+            low_im = high_im = even_im
+        elif even_im is None:
+            low_im, high_im = turn_im, -turn_im
+        else:
+            low_im, high_im = even_im + turn_im, even_im - turn_im
+        low.append((low_re, low_im))
+        high.append((high_re, high_im))
+    return low + high
+
+
+def mixing_kernel(
+    x_ref, pack_ref, cos_ref, sin_ref, table_ref, out_ref,
+    send, held, stack, big, send_back, back, send_sem, recv_sem, send_back_sem, recv_back_sem,
+):
+    bf16, f32 = jnp.bfloat16, jnp.float32
+    seqs, positions, channels = x_ref.shape
+    devices, items, _ = send.shape
+    width = pack_ref.shape[0]
+    groups = channels // width
+    cols = lax.axis_size("col")
+    me = lax.axis_index("row") * cols + lax.axis_index("col")
+    barrier = pltpu.get_barrier_semaphore()
+
+    def peer_of(step):
+        peer = lax.rem(me + step, devices)
+        return peer, (lax.div(peer, cols), lax.rem(peer, cols))
+
+    def greet(step, carry):
+        pl.semaphore_signal(
+            barrier, inc=1, device_id=peer_of(step)[1], device_id_type=pl.DeviceIdType.MESH
+        )
+        return carry
+
+    lax.fori_loop(1, devices, greet, 0)
+    rows_t = (((1,), (1,)), ((), ()))
+    for s in range(seqs):
+        for g in range(groups):
+            lanes = lax.dot_general(
+                pack_ref[...], x_ref[s, :, g * width : (g + 1) * width], rows_t,
+                preferred_element_type=f32,
+            ).astype(bf16)
+            for half in range(2):
+                send[(s * groups + g) * 2 + half] = lanes[half * items : (half + 1) * items]
+    pl.semaphore_wait(barrier, devices - 1)
+
+    def exchange(src, dst, out_sem, in_sem):
+        def copy(step):
+            peer, where = peer_of(step)
+            return pltpu.make_async_remote_copy(
+                src_ref=src.at[peer], dst_ref=dst.at[me], send_sem=out_sem.at[peer],
+                recv_sem=in_sem.at[me], device_id=where, device_id_type=pl.DeviceIdType.MESH,
+            )
+
+        def arrival(step):
+            peer, where = peer_of(step)
+            return pltpu.make_async_remote_copy(
+                src_ref=src.at[peer], dst_ref=dst.at[peer], send_sem=out_sem.at[peer],
+                recv_sem=in_sem.at[peer], device_id=where, device_id_type=pl.DeviceIdType.MESH,
+            )
+
+        def start(step, carry):
+            copy(step).start()
+            return carry
+
+        def finish(step, carry):
+            arrival(step).wait_recv()
+            copy(step).wait_send()
+            return carry
+
+        lax.fori_loop(1, devices, start, 0)
+        dst[me] = src[me]
+        lax.fori_loop(1, devices, finish, 0)
+
+    exchange(send, held, send_sem, recv_sem)
+
+    tile = 16
+    def spin(chunk, carry):
+        rows = pl.ds(pl.multiple_of(chunk * tile, tile), tile)
+        spun = fourier([(held[d, rows, :].astype(f32), None) for d in range(devices)])
+        row_ids = chunk * tile + lax.broadcasted_iota(jnp.int32, (tile, positions), 0)
+        lane_ids = lax.rem(me * items + row_ids, width)
+        is_sine = (lax.rem(lane_ids, 2) == 1) & (lane_ids != 1)
+        for f in range(devices):
+            real_in, imag_in = spun[f]
+            cosine, sine = cos_ref[f : f + 1, :], sin_ref[f : f + 1, :]
+            if imag_in is None:
+                real_part, imag_part = real_in * cosine, -(real_in * sine)
+            else:
+                real_part = real_in * cosine + imag_in * sine
+                imag_part = imag_in * cosine - real_in * sine
+            stack[f, rows, :positions] = jnp.where(is_sine, -imag_part, real_part).astype(bf16)
+            stack[f, rows, positions:] = jnp.where(is_sine, real_part, imag_part).astype(bf16)
+        return carry
+
+    lax.fori_loop(0, items // tile, spin, 0)
+    pairs = devices // 2
+    for a in range(pairs):
+        both = jnp.concatenate([stack[a], stack[a + pairs]], axis=0)
+        big[pl.ds(a, positions, stride=pairs), :] = lax.dot_general(
+            table_ref[...], both, rows_t, preferred_element_type=f32
+        )
+    for e in range(devices):
+        send_back[e] = big[e * items : (e + 1) * items, :].astype(bf16)
+
+    exchange(send_back, back, send_back_sem, recv_back_sem)
+
+    left = lax.broadcasted_iota(jnp.int32, (items, width), 1) < items
+    for s in range(seqs):
+        for g in range(groups):
+            slot = (s * groups + g) * 2
+            first, second = back[slot].astype(f32), back[slot + 1].astype(f32)
+            halves = (
+                jnp.where(left, first, pltpu.roll(second, items, 1)),
+                jnp.where(left, pltpu.roll(first, items, 1), second),
+            )
+            for h in range(2):
+                packed = halves[h].astype(bf16)
+                for m in range(items // pairs):
+                    base = m * devices + h * pairs
+                    out_ref[s, base : base + pairs, g * width : (g + 1) * width] = packed[
+                        m * pairs : (m + 1) * pairs
+                    ]
+
+
+def fused_lanes(mix_input, pack, devices, scale):
     bf16, f32 = jnp.bfloat16, jnp.float32
     seqs, positions, channels = mix_input.shape
-    groups, width, _ = group_maps.shape
-    devices = lax.axis_size("row") * lax.axis_size("col")
-    me = lax.axis_index("row") * lax.axis_size("col") + lax.axis_index("col")
+    width = pack.shape[0]
+    items = seqs * channels // devices
+    length = devices * positions
+    twist_cos, twist_sin = turn_tables(devices, positions, length)
+    pos_cos, pos_sin = turn_tables(positions, positions, positions)
+    table = np.concatenate([pos_cos, pos_sin], axis=1) * scale
+    slots = (devices, items, positions)
+    vmem = pl.BlockSpec(memory_space=pltpu.VMEM)
+    dma = pltpu.SemaphoreType.DMA((devices,))
+    return pl.pallas_call(
+        mixing_kernel,
+        out_shape=jax.ShapeDtypeStruct(mix_input.shape, bf16),
+        in_specs=[vmem] * 5,
+        out_specs=vmem,
+        scratch_shapes=[
+            pltpu.VMEM(slots, bf16), pltpu.VMEM(slots, bf16),
+            pltpu.VMEM((devices, items, 2 * positions), bf16),
+            pltpu.VMEM((devices * items, width), f32),
+            pltpu.VMEM(slots, bf16), pltpu.VMEM(slots, bf16),
+            dma, dma, dma, dma,
+        ],
+        compiler_params=pltpu.CompilerParams(
+            collective_id=0, has_side_effects=True, vmem_limit_bytes=24 * 1024 * 1024
+        ),
+    )(
+        mix_input, jnp.asarray(pack.T, bf16), jnp.asarray(twist_cos, f32),
+        jnp.asarray(twist_sin, f32), jnp.asarray(table, bf16),
+    )
+
+
+def exchanged_lanes(mix_input, pack, width, devices, me, scale):
+    bf16, f32 = jnp.bfloat16, jnp.float32
+    seqs, positions, channels = mix_input.shape
+    groups = channels // width
     length = devices * positions
     items = seqs * channels // devices
-    pack, unpack = lane_tables(width)
-
     lanes = jnp.einsum(
         "spgj,jc->sgcp",
         mix_input.reshape(seqs, positions, groups, width),
@@ -66,7 +245,6 @@
     second = jnp.where(is_sine, real_part, imag_part).astype(bf16)
     stacked = jnp.concatenate([first, second], axis=2)
     pos_cos, pos_sin = turn_tables(positions, positions, positions)
-    scale = 1.0 / math.sqrt(length * width)
     pos_table = jnp.asarray(np.concatenate([pos_cos, pos_sin], axis=0) * scale, bf16)
     freqs = jnp.einsum("pm,fnp->mfn", pos_table, stacked, preferred_element_type=f32).astype(bf16)
 
@@ -74,7 +252,23 @@
     back = lax.all_to_all(freqs, AXES, split_axis=0, concat_axis=0, tiled=True)
     parts = width // items
     back = back.reshape(seqs, groups, parts, positions, items)
-    back = back.transpose(0, 3, 1, 2, 4).reshape(seqs * positions, groups, width)
+    return back.transpose(0, 3, 1, 2, 4).reshape(seqs * positions, groups, width)
+
+
+def per_device(mix_input, group_maps, out_map):
+    bf16, f32 = jnp.bfloat16, jnp.float32
+    seqs, positions, channels = mix_input.shape
+    groups, width, _ = group_maps.shape
+    devices = lax.axis_size("row") * lax.axis_size("col")
+    me = lax.axis_index("row") * lax.axis_size("col") + lax.axis_index("col")
+    items = seqs * channels // devices
+    pack, unpack = lane_tables(width)
+    scale = 1.0 / math.sqrt(devices * positions * width)
+    if 2 * items == width and positions == width and items == 2 * devices:
+        back = fused_lanes(mix_input, pack, devices, scale)
+        back = back.reshape(seqs * positions, groups, width)
+    else:
+        back = exchanged_lanes(mix_input, pack, width, devices, me, scale)
     maps = jnp.einsum(
         "cl,glm->gcm", jnp.asarray(unpack, bf16), group_maps, preferred_element_type=f32
     ).astype(bf16)

time: 55.9 us -> 43.8 us (0.78)
  Pallas kernels: 0 us -> 36 us
  blocking collectives: 18.8 us -> 0 us
  waiting for transfers between devices: 16.2 us -> 0 us
  starting transfers between devices: 7.32 us -> 0 us
  matrix products: 7.93 us -> 3.07 us
  other arithmetic: 0.59 us -> 0 us
    pallas_call x0 -> x1, Pallas kernels: none -> 36 us  [fused_lanes(): pl.pallas_call(mixing_kernel, out_shape=jax.ShapeDtypeStruct(mix_input.sh...]
    all_to_all x1 -> x0, blocking collectives: 18.8 us -> none  [per_device(): back = lax.all_to_all(freqs, AXES, split_axis=0, concat_axis=0, tiled=True)]
    all_to_all x1 -> x0, waiting for transfers between devices: 16.2 us -> none  [per_device(): held = lax.all_to_all(sent, AXES, split_axis=0, concat_axis=0, tiled=True)]
    all_to_all x1 -> x0, starting transfers between devices: 7.32 us -> none  [per_device(): held = lax.all_to_all(sent, AXES, split_axis=0, concat_axis=0, tiled=True)]
    dot_general x3 -> x0, matrix products: 4.85 us -> none  [the longest x1 2.31 us: per_device(): jnp.einsum('spgj,jc->sgcp', mix_input.reshape(seqs, positions, groups, wi...]
    unnamed x14 -> x16, local copies, waits for them, and re-layouts: 0.29 us -> 4.23 us
    convert_element_type x1 -> x0, local copies, waits for them, and re-layouts: 2.46 us -> none  [per_device(): jnp.einsum('pm,fnp->mfn', pos_table, stacked, preferred_element_type=f32)]
    reshape x2 -> x1, local copies, waits for them, and re-layouts: 1.33 us -> 0.12 us  [per_device(): back = back.reshape(seqs * positions, groups, width)]
  transfers between devices with their start and end apart: 1 -> 0, of which waited for: 1 -> 0; matrix products, arithmetic and copies ran while one was open for 0% -> 0% of each run, Pallas kernels for 0% -> 0%
where the time goes in v2:
time: 43.8 us; the launch traced here: 43.4 us
  Pallas kernels  36 us (82%)
  local copies, waits for them, and re-layouts  4.36 us (10%)
  matrix products  3.07 us (7%)
    pallas_call x1, Pallas kernels, fused_lanes(): pl.pallas_call(mixing_kernel, out_shape=jax.ShapeDtypeStruct(mix_input.sh...  36 us
    unnamed x16, local copies, waits for them, and re-layouts  4.23 us
    dot_general x1, matrix products, per_device(): jnp.dot(grouped.reshape(seqs * positions, channels), out_map, preferred_e...  2.59 us

profile of v2, /device:TPU:0, one launch (start us, length us, event | category | flops | bytes accessed | tf_op | source)
XLA Modules:
  0.0 43.4 jit_solution(10942280737605525731)
XLA Ops:
  0.0 0.0 copy-start
  0.0 0.0 copy-start.1
  0.0 1.2 %copy-done.1 = bf16[4,128,512]{2,1,0:T(8,128)(2,1)S(1)} copy-done((bf16[4,128,512]{2,1,0:T(8,128)(2,1)S(1)}, bf16[4,128,512]{2,1,0:T(8,128)(2,1)}, u32[]{:S(2)}) %copy-start.1) | copy-done | bytes 524312
  1.2 0.0 copy-start.2
  1.2 0.8 %copy-done.2 = bf16[128,256]{1,0:T(8,128)(2,1)S(1)} copy-done((bf16[128,256]{1,0:T(8,128)(2,1)S(1)}, bf16[128,256]{1,0:T(8,128)(2,1)}, u32[]{:S(2)}) %copy-start.2) | copy-done | bytes 65560
  2.0 0.0 copy-start.3
  2.0 0.8 %copy-done.3 = bf16[128,128]{1,0:T(8,128)(2,1)S(1)} copy-done((bf16[128,128]{1,0:T(8,128)(2,1)S(1)}, bf16[128,128]{1,0:T(8,128)(2,1)}, u32[]{:S(2)}) %copy-start.3) | copy-done | bytes 32792
  2.8 0.0 copy-start.4
  2.8 0.7 %copy-done.4 = f32[32,128]{1,0:T(8,128)S(1)} copy-done((f32[32,128]{1,0:T(8,128)S(1)}, f32[32,128]{1,0:T(8,128)}, u32[]{:S(2)}) %copy-start.4) | copy-done | bytes 16408
  3.5 0.0 copy-start.5
  3.5 0.7 %copy-done.5 = f32[32,128]{1,0:T(8,128)S(1)} copy-done((f32[32,128]{1,0:T(8,128)S(1)}, f32[32,128]{1,0:T(8,128)}, u32[]{:S(2)}) %copy-start.5) | copy-done | bytes 16408
  4.2 0.0 copy-start.6
  4.2 0.0 copy-start.7
  4.2 36.0 %shard_map.82 = bf16[4,128,512]{2,1,0:T(8,128)(2,1)S(1)} custom-call(bf16[4,128,512]{2,1,0:T(8,128)(2,1)S(1)} %copy-done.1, bf16[128,128]{1,0:T(8,128)(2,1)S(1)} %copy-done.3, f32[32,128]{1,0:T(8,128)S(1)} %copy-done.5, f32[32,128]{1,0:T(8,128)S(1)} %copy-done.4, bf16[128,256]{1,0:T(8,128)(2,1)S(1)} %copy-done.2), custom_call_target="tpu_custom_call" | custom-call | tf_op jit(solution)/shard_map/pallas_call | solution.py:197
  40.2 0.1 reshape.9
  40.3 0.0 copy-done.6
  40.3 0.0 copy-done.7
  40.4 0.5 %convolution_convert_fusion.1 = bf16[4,128,512]{2,1,0:T(8,128)(2,1)S(1)} fusion(bf16[128,128,1]{1,0,2:T(8,128)(2,1)S(1)} %copy-done.7, bf16[4,128,128]{2,1,0:T(8,128)(2,1)S(1)} %copy-done.6, bf16[512,4,128]{2,1,0:T(4,128)(2,1)S(1)} %reshape.9), kind=kOutput, calls=%fused_computation.1 | convolution fusion | flops 84213760 | bytes 1212416 | tf_op jit(solution)/shard_map/rgc,gcm->rgm/dot_general | solution.py:275
  40.8 0.0 copy-done
  40.8 2.6 %convolution_convert_fusion = bf16[512,2048]{1,0:T(8,128)(2,1)} fusion(bf16[512,512]{0,1:T(8,128)(2,1)S(1)} %bitcast.14, bf16[512,2048]{1,0:T(8,128)(2,1)S(1)} %copy-done), kind=kOutput, calls=%fused_computation | convolution fusion | flops 1074790400 | bytes 4718592 | tf_op jit(solution)/shard_map/dot_general | solution.py:276
Async XLA Ops:
  0.0 40.8 %copy-start = (bf16[512,2048]{1,0:T(8,128)(2,1)S(1)}, bf16[512,2048]{1,0:T(8,128)(2,1)}, u32[]{:S(2)}) copy-start(bf16[512,2048]{1,0:T(8,128)(2,1)} %param.10) | copy-start | bytes 6291460
  0.0 1.2 %copy-start.1 = (bf16[4,128,512]{2,1,0:T(8,128)(2,1)S(1)}, bf16[4,128,512]{2,1,0:T(8,128)(2,1)}, u32[]{:S(2)}) copy-start(bf16[4,128,512]{2,1,0:T(8,128)(2,1)} %x_ref.1) | copy-start | bytes 1572868
  1.2 0.8 %copy-start.2 = (bf16[128,256]{1,0:T(8,128)(2,1)S(1)}, bf16[128,256]{1,0:T(8,128)(2,1)}, u32[]{:S(2)}) copy-start(bf16[128,256]{1,0:T(8,128)(2,1)} %constant.13.clone.table_ref) | copy-start | bytes 196612
  2.0 0.8 %copy-start.3 = (bf16[128,128]{1,0:T(8,128)(2,1)S(1)}, bf16[128,128]{1,0:T(8,128)(2,1)}, u32[]{:S(2)}) copy-start(bf16[128,128]{1,0:T(8,128)(2,1)} %constant.10.clone.pack_ref) | copy-start | bytes 98308
  2.8 0.7 %copy-start.4 = (f32[32,128]{1,0:T(8,128)S(1)}, f32[32,128]{1,0:T(8,128)}, u32[]{:S(2)}) copy-start(f32[32,128]{1,0:T(8,128)} %constant.12.clone.sin_ref) | copy-start | bytes 49156
  3.5 0.7 %copy-start.5 = (f32[32,128]{1,0:T(8,128)S(1)}, f32[32,128]{1,0:T(8,128)}, u32[]{:S(2)}) copy-start(f32[32,128]{1,0:T(8,128)} %constant.11.clone.cos_ref) | copy-start | bytes 49156
  4.2 36.1 %copy-start.6 = (bf16[4,128,128]{2,1,0:T(8,128)(2,1)S(1)}, bf16[4,128,128]{2,1,0:T(8,128)(2,1)}, u32[]{:S(2)}) copy-start(bf16[4,128,128]{2,1,0:T(8,128)(2,1)} %param.9) | copy-start | bytes 393220
  4.2 36.1 %copy-start.7 = (bf16[128,128,1]{1,0,2:T(8,128)(2,1)S(1)}, bf16[128,128,1]{1,0,2:T(8,128)(2,1)}, u32[]{:S(2)}) copy-start(bf16[128,128,1]{1,0,2:T(8,128)(2,1)} %constant.15) | copy-start | bytes 98308

commit v3 on v2

--- a/solution.py
+++ b/solution.py
@@ -79,19 +79,34 @@
     groups = channels // width
     cols = lax.axis_size("col")
     me = lax.axis_index("row") * cols + lax.axis_index("col")
+    row, col = lax.axis_index("row"), lax.axis_index("col")
+    row_count, span = devices // cols, cols // 2
+    side = lax.div(col, span)
+    half_count = devices // 2
+    far, near = (0, half_count), (half_count + 1, devices)
     barrier = pltpu.get_barrier_semaphore()
 
     def peer_of(step):
-        peer = lax.rem(me + step, devices)
-        return peer, (lax.div(peer, cols), lax.rem(peer, cols))
-
-    def greet(step, carry):
+        at = lax.rem(step, half_count)
+        peer_side = lax.rem(side + 1 + lax.div(step, half_count), 2)
+        peer_row = lax.rem(row + lax.div(at, span), row_count)
+        peer_col = peer_side * span + lax.rem(col + at, span)
+        return peer_row * cols + peer_col, (peer_row, peer_col)
+
+    def each(steps, act):
+        def body(step, carry):
+            act(step)
+            return carry
+
+        lax.fori_loop(steps[0], steps[1], body, 0)
+
+    def greet(step):
         pl.semaphore_signal(
             barrier, inc=1, device_id=peer_of(step)[1], device_id_type=pl.DeviceIdType.MESH
         )
-        return carry
-
-    lax.fori_loop(1, devices, greet, 0)
+
+    each(far, greet)
+    each(near, greet)
     rows_t = (((1,), (1,)), ((), ()))
     for s in range(seqs):
         for g in range(groups):
@@ -103,35 +118,30 @@
                 send[(s * groups + g) * 2 + half] = lanes[half * items : (half + 1) * items]
     pl.semaphore_wait(barrier, devices - 1)
 
-    def exchange(src, dst, out_sem, in_sem):
-        def copy(step):
-            peer, where = peer_of(step)
-            return pltpu.make_async_remote_copy(
-                src_ref=src.at[peer], dst_ref=dst.at[me], send_sem=out_sem.at[peer],
-                recv_sem=in_sem.at[me], device_id=where, device_id_type=pl.DeviceIdType.MESH,
-            )
-
-        def arrival(step):
-            peer, where = peer_of(step)
-            return pltpu.make_async_remote_copy(
-                src_ref=src.at[peer], dst_ref=dst.at[peer], send_sem=out_sem.at[peer],
-                recv_sem=in_sem.at[peer], device_id=where, device_id_type=pl.DeviceIdType.MESH,
-            )
-
-        def start(step, carry):
-            copy(step).start()
-            return carry
-
-        def finish(step, carry):
-            arrival(step).wait_recv()
-            copy(step).wait_send()
-            return carry
-
-        lax.fori_loop(1, devices, start, 0)
-        dst[me] = src[me]
-        lax.fori_loop(1, devices, finish, 0)
-
-    exchange(send, held, send_sem, recv_sem)
+    def move(src, dst, out_sem, in_sem, step, rows, part, arrives):
+        peer, where = peer_of(step)
+        slot = peer if arrives else me
+        return pltpu.make_async_remote_copy(
+            src_ref=src.at[peer, rows], dst_ref=dst.at[slot, rows],
+            send_sem=out_sem.at[part, peer], recv_sem=in_sem.at[part, slot],
+            device_id=where, device_id_type=pl.DeviceIdType.MESH,
+        )
+
+    chunks = send_sem.shape[0]
+    chunk_rows = items // chunks
+    whole = pl.ds(0, items)
+
+    def outward(part, step, arrives):
+        rows = pl.ds(part * chunk_rows, chunk_rows)
+        return move(send, held, send_sem, recv_sem, step, rows, part, arrives)
+
+    def homeward(step, arrives):
+        return move(send_back, back, send_back_sem, recv_back_sem, step, whole, 0, arrives)
+
+    for part in range(chunks):
+        for steps in (far, near):
+            each(steps, lambda step: outward(part, step, False).start())
+    held[me] = send[me]
 
     tile = 16
     def spin(chunk, carry):
@@ -152,17 +162,33 @@
             stack[f, rows, positions:] = jnp.where(is_sine, real_part, imag_part).astype(bf16)
         return carry
 
-    lax.fori_loop(0, items // tile, spin, 0)
+    for part in range(chunks):
+        for steps in (near, far):
+            each(steps, lambda step: outward(part, step, True).wait_recv())
+        tiles = chunk_rows // tile
+        lax.fori_loop(part * tiles, (part + 1) * tiles, spin, 0)
     pairs = devices // 2
-    for a in range(pairs):
-        both = jnp.concatenate([stack[a], stack[a + pairs]], axis=0)
-        big[pl.ds(a, positions, stride=pairs), :] = lax.dot_general(
-            table_ref[...], both, rows_t, preferred_element_type=f32
-        )
-    for e in range(devices):
-        send_back[e] = big[e * items : (e + 1) * items, :].astype(bf16)
-
-    exchange(send_back, back, send_back_sem, recv_back_sem)
+    group = span * positions // devices
+    for other in (1, 0):
+        half_side = lax.rem(side + other, 2)
+        rows = [
+            table_ref[pl.ds(pl.multiple_of((r * 2 + half_side) * group, group), group), :]
+            for r in range(row_count)
+        ]
+        table = jnp.concatenate(rows, axis=0)
+        for a in range(pairs):
+            both = jnp.concatenate([stack[a], stack[a + pairs]], axis=0)
+            big[other, pl.ds(a, positions // 2, stride=pairs), :] = lax.dot_general(
+                table, both, rows_t, preferred_element_type=f32
+            )
+        for r in range(row_count):
+            for c in range(span):
+                at = (r * span + c) * items
+                send_back[r * cols + half_side * span + c] = big[other, at : at + items, :].astype(bf16)
+        each(far if other else near, lambda step: homeward(step, False).start())
+    back[me] = send_back[me]
+    for steps in (near, far):
+        each(steps, lambda step: homeward(step, True).wait_recv())
 
     left = lax.broadcasted_iota(jnp.int32, (items, width), 1) < items
     for s in range(seqs):
@@ -180,6 +206,10 @@
                     out_ref[s, base : base + pairs, g * width : (g + 1) * width] = packed[
                         m * pairs : (m + 1) * pairs
                     ]
+    for steps in (far, near):
+        for part in range(chunks):
+            each(steps, lambda step: outward(part, step, False).wait_send())
+        each(steps, lambda step: homeward(step, False).wait_send())
 
 
 def fused_lanes(mix_input, pack, devices, scale):
@@ -193,7 +223,7 @@
     table = np.concatenate([pos_cos, pos_sin], axis=1) * scale
     slots = (devices, items, positions)
     vmem = pl.BlockSpec(memory_space=pltpu.VMEM)
-    dma = pltpu.SemaphoreType.DMA((devices,))
+    dma, dma_back = pltpu.SemaphoreType.DMA((2, devices)), pltpu.SemaphoreType.DMA((1, devices))
     return pl.pallas_call(
         mixing_kernel,
         out_shape=jax.ShapeDtypeStruct(mix_input.shape, bf16),
@@ -202,9 +232,9 @@
         scratch_shapes=[
             pltpu.VMEM(slots, bf16), pltpu.VMEM(slots, bf16),
             pltpu.VMEM((devices, items, 2 * positions), bf16),
-            pltpu.VMEM((devices * items, width), f32),
+            pltpu.VMEM((2, devices * items // 2, width), f32),
             pltpu.VMEM(slots, bf16), pltpu.VMEM(slots, bf16),
-            dma, dma, dma, dma,
+            dma, dma, dma_back, dma_back,
         ],
         compiler_params=pltpu.CompilerParams(
             collective_id=0, has_side_effects=True, vmem_limit_bytes=24 * 1024 * 1024
@@ -264,7 +294,8 @@
     items = seqs * channels // devices
     pack, unpack = lane_tables(width)
     scale = 1.0 / math.sqrt(devices * positions * width)
-    if 2 * items == width and positions == width and items == 2 * devices:
+    fits = 2 * items == width and positions == width and items == 2 * devices
+    if fits and lax.axis_size("col") * positions == 32 * devices:
         back = fused_lanes(mix_input, pack, devices, scale)
         back = back.reshape(seqs * positions, groups, width)
     else:

time: 43.8 us -> 46.3 us (1.057)
  Pallas kernels: 36 us -> 38.5 us
    pallas_call x1, Pallas kernels: 36 us -> 38.5 us  [fused_lanes(): pl.pallas_call(mixing_kernel, out_shape=jax.ShapeDtypeStruct(mix_input.sh...]
where the time goes in v3:
time: 46.3 us; the launch traced here: 46 us
  Pallas kernels  38.5 us (83%)
  local copies, waits for them, and re-layouts  4.36 us (9%)
  matrix products  3.07 us (7%)
    pallas_call x1, Pallas kernels, fused_lanes(): pl.pallas_call(mixing_kernel, out_shape=jax.ShapeDtypeStruct(mix_input.sh...  38.5 us
    unnamed x16, local copies, waits for them, and re-layouts  4.23 us
    dot_general x1, matrix products, per_device(): jnp.dot(grouped.reshape(seqs * positions, channels), out_map, preferred_e...  2.59 us

profile of v3, /device:TPU:0, one launch (start us, length us, event | category | flops | bytes accessed | tf_op | source)
XLA Modules:
  0.0 46.0 jit_solution(15325275098948795535)
XLA Ops:
  0.0 0.0 copy-start
  0.0 0.0 copy-start.1
  0.0 1.2 %copy-done.1 = bf16[4,128,512]{2,1,0:T(8,128)(2,1)S(1)} copy-done((bf16[4,128,512]{2,1,0:T(8,128)(2,1)S(1)}, bf16[4,128,512]{2,1,0:T(8,128)(2,1)}, u32[]{:S(2)}) %copy-start.1) | copy-done | bytes 524312
  1.2 0.0 copy-start.2
  1.2 0.8 %copy-done.2 = bf16[128,256]{1,0:T(8,128)(2,1)S(1)} copy-done((bf16[128,256]{1,0:T(8,128)(2,1)S(1)}, bf16[128,256]{1,0:T(8,128)(2,1)}, u32[]{:S(2)}) %copy-start.2) | copy-done | bytes 65560
  2.0 0.0 copy-start.3
  2.0 0.8 %copy-done.3 = bf16[128,128]{1,0:T(8,128)(2,1)S(1)} copy-done((bf16[128,128]{1,0:T(8,128)(2,1)S(1)}, bf16[128,128]{1,0:T(8,128)(2,1)}, u32[]{:S(2)}) %copy-start.3) | copy-done | bytes 32792
  2.8 0.0 copy-start.4
  2.8 0.7 %copy-done.4 = f32[32,128]{1,0:T(8,128)S(1)} copy-done((f32[32,128]{1,0:T(8,128)S(1)}, f32[32,128]{1,0:T(8,128)}, u32[]{:S(2)}) %copy-start.4) | copy-done | bytes 16408
  3.5 0.0 copy-start.5
  3.5 0.7 %copy-done.5 = f32[32,128]{1,0:T(8,128)S(1)} copy-done((f32[32,128]{1,0:T(8,128)S(1)}, f32[32,128]{1,0:T(8,128)}, u32[]{:S(2)}) %copy-start.5) | copy-done | bytes 16408
  4.2 0.0 copy-start.6
  4.2 0.0 copy-start.7
  4.2 38.5 %shard_map.82 = bf16[4,128,512]{2,1,0:T(8,128)(2,1)S(1)} custom-call(bf16[4,128,512]{2,1,0:T(8,128)(2,1)S(1)} %copy-done.1, bf16[128,128]{1,0:T(8,128)(2,1)S(1)} %copy-done.3, f32[32,128]{1,0:T(8,128)S(1)} %copy-done.5, f32[32,128]{1,0:T(8,128)S(1)} %copy-done.4, bf16[128,256]{1,0:T(8,128)(2,1)S(1)} %copy-done.2), custom_call_target="tpu_custom_call" | custom-call | tf_op jit(solution)/shard_map/pallas_call | solution.py:227
  42.7 0.1 reshape.9
  42.9 0.0 copy-done.6
  42.9 0.0 copy-done.7
  42.9 0.5 %convolution_convert_fusion.1 = bf16[4,128,512]{2,1,0:T(8,128)(2,1)S(1)} fusion(bf16[128,128,1]{1,0,2:T(8,128)(2,1)S(1)} %copy-done.7, bf16[4,128,128]{2,1,0:T(8,128)(2,1)S(1)} %copy-done.6, bf16[512,4,128]{2,1,0:T(4,128)(2,1)S(1)} %reshape.9), kind=kOutput, calls=%fused_computation.1 | convolution fusion | flops 84213760 | bytes 1212416 | tf_op jit(solution)/shard_map/rgc,gcm->rgm/dot_general | solution.py:306
  43.4 0.0 copy-done
  43.4 2.6 %convolution_convert_fusion = bf16[512,2048]{1,0:T(8,128)(2,1)} fusion(bf16[512,512]{0,1:T(8,128)(2,1)S(1)} %bitcast.14, bf16[512,2048]{1,0:T(8,128)(2,1)S(1)} %copy-done), kind=kOutput, calls=%fused_computation | convolution fusion | flops 1074790400 | bytes 4718592 | tf_op jit(solution)/shard_map/dot_general | solution.py:307
Async XLA Ops:
  0.0 43.4 %copy-start = (bf16[512,2048]{1,0:T(8,128)(2,1)S(1)}, bf16[512,2048]{1,0:T(8,128)(2,1)}, u32[]{:S(2)}) copy-start(bf16[512,2048]{1,0:T(8,128)(2,1)} %param.10) | copy-start | bytes 6291460
  0.0 1.2 %copy-start.1 = (bf16[4,128,512]{2,1,0:T(8,128)(2,1)S(1)}, bf16[4,128,512]{2,1,0:T(8,128)(2,1)}, u32[]{:S(2)}) copy-start(bf16[4,128,512]{2,1,0:T(8,128)(2,1)} %x_ref.1) | copy-start | bytes 1572868
  1.2 0.8 %copy-start.2 = (bf16[128,256]{1,0:T(8,128)(2,1)S(1)}, bf16[128,256]{1,0:T(8,128)(2,1)}, u32[]{:S(2)}) copy-start(bf16[128,256]{1,0:T(8,128)(2,1)} %constant.13.clone.table_ref) | copy-start | bytes 196612
  2.0 0.8 %copy-start.3 = (bf16[128,128]{1,0:T(8,128)(2,1)S(1)}, bf16[128,128]{1,0:T(8,128)(2,1)}, u32[]{:S(2)}) copy-start(bf16[128,128]{1,0:T(8,128)(2,1)} %constant.10.clone.pack_ref) | copy-start | bytes 98308
  2.8 0.7 %copy-start.4 = (f32[32,128]{1,0:T(8,128)S(1)}, f32[32,128]{1,0:T(8,128)}, u32[]{:S(2)}) copy-start(f32[32,128]{1,0:T(8,128)} %constant.12.clone.sin_ref) | copy-start | bytes 49156
  3.5 0.7 %copy-start.5 = (f32[32,128]{1,0:T(8,128)S(1)}, f32[32,128]{1,0:T(8,128)}, u32[]{:S(2)}) copy-start(f32[32,128]{1,0:T(8,128)} %constant.11.clone.cos_ref) | copy-start | bytes 49156
  4.2 38.6 %copy-start.6 = (bf16[4,128,128]{2,1,0:T(8,128)(2,1)S(1)}, bf16[4,128,128]{2,1,0:T(8,128)(2,1)}, u32[]{:S(2)}) copy-start(bf16[4,128,128]{2,1,0:T(8,128)(2,1)} %param.9) | copy-start | bytes 393220
  4.2 38.7 %copy-start.7 = (bf16[128,128,1]{1,0,2:T(8,128)(2,1)S(1)}, bf16[128,128,1]{1,0,2:T(8,128)(2,1)}, u32[]{:S(2)}) copy-start(bf16[128,128,1]{1,0,2:T(8,128)(2,1)} %constant.15) | copy-start | bytes 98308

commit v4 on v2

--- a/solution.py
+++ b/solution.py
@@ -69,7 +69,8 @@
 
 
 def mixing_kernel(
-    x_ref, pack_ref, cos_ref, sin_ref, table_ref, out_ref,
+    x_hbm, pack_hbm, cos_hbm, sin_hbm, table_hbm, out_ref,
+    x_ref, pack_ref, cos_ref, sin_ref, table_ref, load_sem,
     send, held, stack, big, send_back, back, send_sem, recv_sem, send_back_sem, recv_back_sem,
 ):
     bf16, f32 = jnp.bfloat16, jnp.float32
@@ -79,6 +80,14 @@
     groups = channels // width
     cols = lax.axis_size("col")
     me = lax.axis_index("row") * cols + lax.axis_index("col")
+    far_refs = (x_hbm, pack_hbm, cos_hbm, sin_hbm, table_hbm)
+    near_refs = (x_ref, pack_ref, cos_ref, sin_ref, table_ref)
+    loads = [
+        pltpu.make_async_copy(src, dst, load_sem.at[at])
+        for at, (src, dst) in enumerate(zip(far_refs, near_refs))
+    ]
+    for load in loads:
+        load.start()
     barrier = pltpu.get_barrier_semaphore()
 
     def peer_of(step):
@@ -93,6 +102,8 @@
 
     lax.fori_loop(1, devices, greet, 0)
     rows_t = (((1,), (1,)), ((), ()))
+    loads[0].wait()
+    loads[1].wait()
     for s in range(seqs):
         for g in range(groups):
             lanes = lax.dot_general(
@@ -132,6 +143,8 @@
         lax.fori_loop(1, devices, finish, 0)
 
     exchange(send, held, send_sem, recv_sem)
+    for load in loads[2:]:
+        load.wait()
 
     tile = 16
     def spin(chunk, carry):
@@ -193,13 +206,17 @@
     table = np.concatenate([pos_cos, pos_sin], axis=1) * scale
     slots = (devices, items, positions)
     vmem = pl.BlockSpec(memory_space=pltpu.VMEM)
+    hbm = pl.BlockSpec(memory_space=pltpu.HBM)
     dma = pltpu.SemaphoreType.DMA((devices,))
     return pl.pallas_call(
         mixing_kernel,
         out_shape=jax.ShapeDtypeStruct(mix_input.shape, bf16),
-        in_specs=[vmem] * 5,
+        in_specs=[hbm] * 5,
         out_specs=vmem,
         scratch_shapes=[
+            pltpu.VMEM(mix_input.shape, bf16), pltpu.VMEM(pack.shape, bf16),
+            pltpu.VMEM(twist_cos.shape, f32), pltpu.VMEM(twist_sin.shape, f32),
+            pltpu.VMEM(table.shape, bf16), pltpu.SemaphoreType.DMA((5,)),
             pltpu.VMEM(slots, bf16), pltpu.VMEM(slots, bf16),
             pltpu.VMEM((devices, items, 2 * positions), bf16),
             pltpu.VMEM((devices * items, width), f32),
@@ -207,7 +224,7 @@
             dma, dma, dma, dma,
         ],
         compiler_params=pltpu.CompilerParams(
-            collective_id=0, has_side_effects=True, vmem_limit_bytes=24 * 1024 * 1024
+            collective_id=0, has_side_effects=True
         ),
     )(
         mix_input, jnp.asarray(pack.T, bf16), jnp.asarray(twist_cos, f32),

time: 43.8 us -> 41.4 us (0.945)
  local copies, waits for them, and re-layouts: 4.36 us -> 1.18 us
  Pallas kernels: 36 us -> 36.9 us
    unnamed x16 -> x6, local copies, waits for them, and re-layouts: 4.23 us -> 0.01 us
    reshape x1, local copies, waits for them, and re-layouts: 0.12 us -> 1.16 us  [per_device(): back = back.reshape(seqs * positions, groups, width)]
    pallas_call x1, Pallas kernels: 36 us -> 36.9 us  [fused_lanes(): pl.pallas_call(mixing_kernel, out_shape=jax.ShapeDtypeStruct(mix_input.sh...]
where the time goes in v4:
time: 41.4 us; the launch traced here: 41.2 us
  Pallas kernels  36.9 us (89%)
  matrix products  3.07 us (7%)
  local copies, waits for them, and re-layouts  1.18 us (3%)
    pallas_call x1, Pallas kernels, fused_lanes(): pl.pallas_call(mixing_kernel, out_shape=jax.ShapeDtypeStruct(mix_input.sh...  36.9 us
    dot_general x1, matrix products, per_device(): jnp.dot(grouped.reshape(seqs * positions, channels), out_map, preferred_e...  2.59 us
    reshape x1, local copies, waits for them, and re-layouts, per_device(): back = back.reshape(seqs * positions, groups, width)  1.16 us

profile of v4, /device:TPU:0, one launch (start us, length us, event | category | flops | bytes accessed | tf_op | source)
XLA Modules:
  0.0 41.2 jit_solution(7887522268527574489)
XLA Ops:
  0.0 0.0 copy-start
  0.0 0.0 copy-start.2
  0.0 0.0 copy-start.1
  0.0 36.9 %shard_map.82 = bf16[4,128,512]{2,1,0:T(8,128)(2,1)} custom-call(bf16[4,128,512]{2,1,0:T(8,128)(2,1)} %x_hbm.1, bf16[128,128]{1,0:T(8,128)(2,1)} %constant.10.clone.pack_hbm, f32[32,128]{1,0:T(8,128)} %constant.11.clone.cos_hbm, f32[32,128]{1,0:T(8,128)} %constant.12.clone.sin_hbm, bf16[128,256]{1,0:T(8,128)(2,1)} %constant.13.clone.table_hbm), custom_call_target="tpu_custom_call" | custom-call | tf_op jit(solution)/shard_map/pallas_call | solution.py:211
  36.9 1.2 %reshape.9 = bf16[512,4,128]{2,1,0:T(4,128)(2,1)S(1)} reshape(bf16[4,128,512]{2,1,0:T(8,128)(2,1)} %shard_map.82) | data formatting | bytes 1048576 | tf_op jit(solution)/shard_map/reshape | solution.py:286
  38.1 0.0 copy-done.2
  38.1 0.0 copy-done.1
  38.1 0.5 %convolution_convert_fusion.1 = bf16[4,128,512]{2,1,0:T(8,128)(2,1)S(1)} fusion(bf16[128,128,1]{1,0,2:T(8,128)(2,1)S(1)} %copy-done.2, bf16[4,128,128]{2,1,0:T(8,128)(2,1)S(1)} %copy-done.1, bf16[512,4,128]{2,1,0:T(4,128)(2,1)S(1)} %reshape.9), kind=kOutput, calls=%fused_computation.1 | convolution fusion | flops 84213760 | bytes 1212416 | tf_op jit(solution)/shard_map/rgc,gcm->rgm/dot_general | solution.py:292
  38.6 0.0 copy-done
  38.6 2.6 %convolution_convert_fusion = bf16[512,2048]{1,0:T(8,128)(2,1)} fusion(bf16[512,512]{0,1:T(8,128)(2,1)S(1)} %bitcast.14, bf16[512,2048]{1,0:T(8,128)(2,1)S(1)} %copy-done), kind=kOutput, calls=%fused_computation | convolution fusion | flops 1074790400 | bytes 4718592 | tf_op jit(solution)/shard_map/dot_general | solution.py:293
Async XLA Ops:
  0.0 38.6 %copy-start = (bf16[512,2048]{1,0:T(8,128)(2,1)S(1)}, bf16[512,2048]{1,0:T(8,128)(2,1)}, u32[]{:S(2)}) copy-start(bf16[512,2048]{1,0:T(8,128)(2,1)} %param.10) | copy-start | bytes 6291460
  0.0 38.1 %copy-start.2 = (bf16[128,128,1]{1,0,2:T(8,128)(2,1)S(1)}, bf16[128,128,1]{1,0,2:T(8,128)(2,1)}, u32[]{:S(2)}) copy-start(bf16[128,128,1]{1,0,2:T(8,128)(2,1)} %constant.15) | copy-start | bytes 98308
  0.0 38.1 %copy-start.1 = (bf16[4,128,128]{2,1,0:T(8,128)(2,1)S(1)}, bf16[4,128,128]{2,1,0:T(8,128)(2,1)}, u32[]{:S(2)}) copy-start(bf16[4,128,128]{2,1,0:T(8,128)(2,1)} %param.9) | copy-start | bytes 393220

commit v5 on v4

--- a/solution.py
+++ b/solution.py
@@ -69,8 +69,8 @@
 
 
 def mixing_kernel(
-    x_hbm, pack_hbm, cos_hbm, sin_hbm, table_hbm, out_ref,
-    x_ref, pack_ref, cos_ref, sin_ref, table_ref, load_sem,
+    x_hbm, pack_hbm, cos_hbm, sin_hbm, table_hbm, unpack_hbm, given_hbm, out_ref,
+    x_ref, pack_ref, cos_ref, sin_ref, table_ref, unpack_ref, given_ref, maps, load_sem,
     send, held, stack, big, send_back, back, send_sem, recv_sem, send_back_sem, recv_back_sem,
 ):
     bf16, f32 = jnp.bfloat16, jnp.float32
@@ -80,8 +80,8 @@
     groups = channels // width
     cols = lax.axis_size("col")
     me = lax.axis_index("row") * cols + lax.axis_index("col")
-    far_refs = (x_hbm, pack_hbm, cos_hbm, sin_hbm, table_hbm)
-    near_refs = (x_ref, pack_ref, cos_ref, sin_ref, table_ref)
+    far_refs = (x_hbm, pack_hbm, cos_hbm, sin_hbm, table_hbm, unpack_hbm, given_hbm)
+    near_refs = (x_ref, pack_ref, cos_ref, sin_ref, table_ref, unpack_ref, given_ref)
     loads = [
         pltpu.make_async_copy(src, dst, load_sem.at[at])
         for at, (src, dst) in enumerate(zip(far_refs, near_refs))
@@ -114,7 +114,7 @@
                 send[(s * groups + g) * 2 + half] = lanes[half * items : (half + 1) * items]
     pl.semaphore_wait(barrier, devices - 1)
 
-    def exchange(src, dst, out_sem, in_sem):
+    def exchange(src, dst, out_sem, in_sem, beside):
         def copy(step):
             peer, where = peer_of(step)
             return pltpu.make_async_remote_copy(
@@ -140,11 +140,18 @@
 
         lax.fori_loop(1, devices, start, 0)
         dst[me] = src[me]
+        beside()
         lax.fori_loop(1, devices, finish, 0)
 
-    exchange(send, held, send_sem, recv_sem)
-    for load in loads[2:]:
-        load.wait()
+    def ready_maps():
+        for load in loads[2:]:
+            load.wait()
+        for g in range(groups):
+            maps[g] = jnp.dot(
+                unpack_ref[...], given_ref[g], preferred_element_type=f32
+            ).astype(bf16)
+
+    exchange(send, held, send_sem, recv_sem, ready_maps)
 
     tile = 16
     def spin(chunk, carry):
@@ -175,7 +182,7 @@
     for e in range(devices):
         send_back[e] = big[e * items : (e + 1) * items, :].astype(bf16)
 
-    exchange(send_back, back, send_back_sem, recv_back_sem)
+    exchange(send_back, back, send_back_sem, recv_back_sem, lambda: None)
 
     left = lax.broadcasted_iota(jnp.int32, (items, width), 1) < items
     for s in range(seqs):
@@ -187,7 +194,9 @@
                 jnp.where(left, pltpu.roll(first, items, 1), second),
             )
             for h in range(2):
-                packed = halves[h].astype(bf16)
+                packed = jnp.dot(
+                    halves[h].astype(bf16), maps[g], preferred_element_type=f32
+                ).astype(bf16)
                 for m in range(items // pairs):
                     base = m * devices + h * pairs
                     out_ref[s, base : base + pairs, g * width : (g + 1) * width] = packed[
@@ -195,7 +204,7 @@
                     ]
 
 
-def fused_lanes(mix_input, pack, devices, scale):
+def fused_lanes(mix_input, group_maps, pack, unpack, devices, scale):
     bf16, f32 = jnp.bfloat16, jnp.float32
     seqs, positions, channels = mix_input.shape
     width = pack.shape[0]
@@ -211,12 +220,14 @@
     return pl.pallas_call(
         mixing_kernel,
         out_shape=jax.ShapeDtypeStruct(mix_input.shape, bf16),
-        in_specs=[hbm] * 5,
+        in_specs=[hbm] * 7,
         out_specs=vmem,
         scratch_shapes=[
             pltpu.VMEM(mix_input.shape, bf16), pltpu.VMEM(pack.shape, bf16),
             pltpu.VMEM(twist_cos.shape, f32), pltpu.VMEM(twist_sin.shape, f32),
-            pltpu.VMEM(table.shape, bf16), pltpu.SemaphoreType.DMA((5,)),
+            pltpu.VMEM(table.shape, bf16), pltpu.VMEM(unpack.shape, bf16),
+            pltpu.VMEM(group_maps.shape, bf16), pltpu.VMEM(group_maps.shape, bf16),
+            pltpu.SemaphoreType.DMA((7,)),
             pltpu.VMEM(slots, bf16), pltpu.VMEM(slots, bf16),
             pltpu.VMEM((devices, items, 2 * positions), bf16),
             pltpu.VMEM((devices * items, width), f32),
@@ -228,7 +239,7 @@
         ),
     )(
         mix_input, jnp.asarray(pack.T, bf16), jnp.asarray(twist_cos, f32),
-        jnp.asarray(twist_sin, f32), jnp.asarray(table, bf16),
+        jnp.asarray(twist_sin, f32), jnp.asarray(table, bf16), jnp.asarray(unpack, bf16), group_maps,
     )
 
 
@@ -282,14 +293,13 @@
     pack, unpack = lane_tables(width)
     scale = 1.0 / math.sqrt(devices * positions * width)
     if 2 * items == width and positions == width and items == 2 * devices:
-        back = fused_lanes(mix_input, pack, devices, scale)
-        back = back.reshape(seqs * positions, groups, width)
+        grouped = fused_lanes(mix_input, group_maps, pack, unpack, devices, scale)
     else:
         back = exchanged_lanes(mix_input, pack, width, devices, me, scale)
-    maps = jnp.einsum(
-        "cl,glm->gcm", jnp.asarray(unpack, bf16), group_maps, preferred_element_type=f32
-    ).astype(bf16)
-    grouped = jnp.einsum("rgc,gcm->rgm", back, maps, preferred_element_type=f32).astype(bf16)
+        maps = jnp.einsum(
+            "cl,glm->gcm", jnp.asarray(unpack, bf16), group_maps, preferred_element_type=f32
+        ).astype(bf16)
+        grouped = jnp.einsum("rgc,gcm->rgm", back, maps, preferred_element_type=f32).astype(bf16)
     mixed = jnp.dot(
         grouped.reshape(seqs * positions, channels), out_map, preferred_element_type=f32
     )

time: 41.4 us -> 41 us (level)
  local copies, waits for them, and re-layouts: 1.18 us -> 0.01 us
  matrix products: 3.07 us -> 3.62 us
    reshape x1 -> x0, local copies, waits for them, and re-layouts: 1.16 us -> none  [per_device(): back = back.reshape(seqs * positions, groups, width)]
    dot_general x1, matrix products: 2.59 us -> 3.62 us  [per_device(): jnp.dot(grouped.reshape(seqs * positions, channels), out_map, preferred_e...]
    dot_general x1 -> x0, matrix products: 0.48 us -> none  [per_device(): jnp.einsum('rgc,gcm->rgm', back, maps, preferred_element_type=f32)]
where the time goes in v5:
time: 41 us; the launch traced here: 40.8 us
  Pallas kernels  37.2 us (91%)
  matrix products  3.62 us (9%)
    pallas_call x1, Pallas kernels, fused_lanes(): pl.pallas_call(mixing_kernel, out_shape=jax.ShapeDtypeStruct(mix_input.sh...  37.2 us
    dot_general x1, matrix products, per_device(): jnp.dot(grouped.reshape(seqs * positions, channels), out_map, preferred_e...  3.62 us

profile of v5, /device:TPU:0, one launch (start us, length us, event | category | flops | bytes accessed | tf_op | source)
XLA Modules:
  0.0 40.8 jit_solution(16398621087362191236)
XLA Ops:
  0.0 0.0 copy-start
  0.0 37.2 %shard_map.82 = bf16[4,128,512]{2,1,0:T(8,128)(2,1)} custom-call(bf16[4,128,512]{2,1,0:T(8,128)(2,1)} %x_hbm.1, bf16[128,128]{1,0:T(8,128)(2,1)} %constant.10.clone.pack_hbm, f32[32,128]{1,0:T(8,128)} %constant.11.clone.cos_hbm, f32[32,128]{1,0:T(8,128)} %constant.12.clone.sin_hbm, bf16[128,256]{1,0:T(8,128)(2,1)} %constant.13.clone.table_hbm, ...), custom_call_target="tpu_custom_call" | custom-call | tf_op jit(solution)/shard_map/pallas_call | solution.py:220
  37.2 0.0 copy-done
  37.2 3.6 %convolution_convert_fusion = bf16[512,2048]{1,0:T(8,128)(2,1)} fusion(bf16[512,512]{1,0:T(8,128)(2,1)} %bitcast.4, bf16[512,2048]{1,0:T(8,128)(2,1)S(1)} %copy-done), kind=kOutput, calls=%fused_computation | convolution fusion | flops 1074790400 | bytes 4718592 | tf_op jit(solution)/shard_map/dot_general | solution.py:303
Async XLA Ops:
  0.0 37.2 %copy-start = (bf16[512,2048]{1,0:T(8,128)(2,1)S(1)}, bf16[512,2048]{1,0:T(8,128)(2,1)}, u32[]{:S(2)}) copy-start(bf16[512,2048]{1,0:T(8,128)(2,1)} %param.10) | copy-start | bytes 6291460

commit v6 on v5

--- a/solution.py
+++ b/solution.py
@@ -141,7 +141,7 @@
         lax.fori_loop(1, devices, start, 0)
         dst[me] = src[me]
         beside()
-        lax.fori_loop(1, devices, finish, 0)
+        return copy, arrival, finish
 
     def ready_maps():
         for load in loads[2:]:
@@ -151,7 +151,8 @@
                 unpack_ref[...], given_ref[g], preferred_element_type=f32
             ).astype(bf16)
 
-    exchange(send, held, send_sem, recv_sem, ready_maps)
+    finish = exchange(send, held, send_sem, recv_sem, ready_maps)[2]
+    lax.fori_loop(1, devices, finish, 0)
 
     tile = 16
     def spin(chunk, carry):
@@ -182,26 +183,41 @@
     for e in range(devices):
         send_back[e] = big[e * items : (e + 1) * items, :].astype(bf16)
 
-    exchange(send_back, back, send_back_sem, recv_back_sem, lambda: None)
+    copy, arrival, _ = exchange(send_back, back, send_back_sem, recv_back_sem, lambda: None)
 
     left = lax.broadcasted_iota(jnp.int32, (items, width), 1) < items
-    for s in range(seqs):
-        for g in range(groups):
-            slot = (s * groups + g) * 2
-            first, second = back[slot].astype(f32), back[slot + 1].astype(f32)
-            halves = (
-                jnp.where(left, first, pltpu.roll(second, items, 1)),
-                jnp.where(left, pltpu.roll(first, items, 1), second),
-            )
-            for h in range(2):
-                packed = jnp.dot(
-                    halves[h].astype(bf16), maps[g], preferred_element_type=f32
-                ).astype(bf16)
-                for m in range(items // pairs):
-                    base = m * devices + h * pairs
-                    out_ref[s, base : base + pairs, g * width : (g + 1) * width] = packed[
-                        m * pairs : (m + 1) * pairs
-                    ]
+    def settle(at, carry):
+        pair = lax.rem(lax.div(me, 2) + pairs - at, pairs)
+        slot = pair * 2
+        for source in (slot, slot + 1):
+
+            @pl.when(source != me)
+            def _():
+                arrival(lax.rem(source + devices - me, devices)).wait_recv()
+
+        s, g = lax.div(pair, groups), lax.rem(pair, groups)
+        lanes_at = pl.ds(pl.multiple_of(g * width, width), width)
+        first, second = back[slot].astype(f32), back[slot + 1].astype(f32)
+        halves = (
+            jnp.where(left, first, pltpu.roll(second, items, 1)),
+            jnp.where(left, pltpu.roll(first, items, 1), second),
+        )
+        for h in range(2):
+            packed = jnp.dot(
+                halves[h].astype(bf16), maps[g], preferred_element_type=f32
+            ).astype(bf16)
+            for m in range(items // pairs):
+                base = m * devices + h * pairs
+                out_ref[s, base : base + pairs, lanes_at] = packed[m * pairs : (m + 1) * pairs]
+        return carry
+
+    lax.fori_loop(0, pairs, settle, 0)
+
+    def sent(step, carry):
+        copy(step).wait_send()
+        return carry
+
+    lax.fori_loop(1, devices, sent, 0)
 
 
 def fused_lanes(mix_input, group_maps, pack, unpack, devices, scale):

time: 41 us -> 41.4 us (level)
    pallas_call x1, Pallas kernels: 37.2 us -> 37.6 us  [fused_lanes(): pl.pallas_call(mixing_kernel, out_shape=jax.ShapeDtypeStruct(mix_input.sh...]
where the time goes in v6:
time: 41.4 us; the launch traced here: 41.2 us
  Pallas kernels  37.6 us (91%)
  matrix products  3.62 us (9%)
    pallas_call x1, Pallas kernels, fused_lanes(): pl.pallas_call(mixing_kernel, out_shape=jax.ShapeDtypeStruct(mix_input.sh...  37.6 us
    dot_general x1, matrix products, per_device(): jnp.dot(grouped.reshape(seqs * positions, channels), out_map, preferred_e...  3.62 us

profile of v6, /device:TPU:0, one launch (start us, length us, event | category | flops | bytes accessed | tf_op | source)
XLA Modules:
  0.0 41.2 jit_solution(7342153598375327144)
XLA Ops:
  0.0 0.0 copy-start
  0.0 37.6 %shard_map.82 = bf16[4,128,512]{2,1,0:T(8,128)(2,1)} custom-call(bf16[4,128,512]{2,1,0:T(8,128)(2,1)} %x_hbm.1, bf16[128,128]{1,0:T(8,128)(2,1)} %constant.10.clone.pack_hbm, f32[32,128]{1,0:T(8,128)} %constant.11.clone.cos_hbm, f32[32,128]{1,0:T(8,128)} %constant.12.clone.sin_hbm, bf16[128,256]{1,0:T(8,128)(2,1)} %constant.13.clone.table_hbm, ...), custom_call_target="tpu_custom_call" | custom-call | tf_op jit(solution)/shard_map/pallas_call | solution.py:236
  37.6 0.0 copy-done
  37.6 3.6 %convolution_convert_fusion = bf16[512,2048]{1,0:T(8,128)(2,1)} fusion(bf16[512,512]{1,0:T(8,128)(2,1)} %bitcast.4, bf16[512,2048]{1,0:T(8,128)(2,1)S(1)} %copy-done), kind=kOutput, calls=%fused_computation | convolution fusion | flops 1074790400 | bytes 4718592 | tf_op jit(solution)/shard_map/dot_general | solution.py:319
Async XLA Ops:
  0.0 37.6 %copy-start = (bf16[512,2048]{1,0:T(8,128)(2,1)S(1)}, bf16[512,2048]{1,0:T(8,128)(2,1)}, u32[]{:S(2)}) copy-start(bf16[512,2048]{1,0:T(8,128)(2,1)} %param.10) | copy-start | bytes 6291460
